TPU v7x, 512 devices: a whole 4x8x8 slice. The times are simulated.
512 devices in a mesh: sp: 64 (over z, y), fs: 4 (over x), tp: 2 (over core).
Axes of the slice: x: 4, y: 8, z: 8, core: 2. Of those that a mesh axis runs over, the one named last changes fastest.
Arguments:
- tokens: bfloat16 [16384, 2048], P(('sp', 'fs', 'tp')), may hold values from -6 to 6
- norm_gain: float32 [2048], replicated, may hold values from 0.1 to 1.9
- w_query: bfloat16 [2048, 2048], P(None, ('fs', 'tp')), may hold values from -0.9722718 to 0.9722718
- w_key: bfloat16 [2048, 512], P(None, 'fs'), may hold values from -0.77339804 to 0.77339804
- w_value: bfloat16 [2048, 512], P(None, 'fs'), may hold values from -0.125 to 0.125
- w_conv_value: bfloat16 [2048, 1024], P(None, ('fs', 'tp')), may hold values from -0.125 to 0.125
- w_conv_pre: bfloat16 [2048, 1024], P(None, ('fs', 'tp')), may hold values from -0.125 to 0.125
- w_conv_post: bfloat16 [2048, 1024], P(None, ('fs', 'tp')), may hold values from -0.125 to 0.125
- conv_taps: bfloat16 [3, 1024], replicated, may hold values from -3.5 to 3.5
- log_gate_cache: float32 [16, 16384], replicated, may hold values from -987 to 0, as said below
- w_out_conv: bfloat16 [1024, 2048], P(('fs', 'tp')), may hold values from -0.125 to 0.125
- w_out_attn: bfloat16 [2048, 2048], P(('fs', 'tp')), may hold values from -0.375 to 0.375
Outputs:
- mixed: bfloat16 [16384, 2048], P(('sp', 'fs', 'tp'))
Inputs may be any that keep to these rules, and one draw needn't show every extreme that they name: `log_gate_cache`: each row is a cumulative sum over positions of log forget gates, none of them positive.
All inputs are finite; a program needn't handle non-finite values.
Results may differ from a plain program's by a relative error of at most 0.014.
The roundings to bfloat16 on the way count: a program that leaves them out, or rounds other values in their place, can miss the bound.
Values may be sent and summed in bfloat16 or wider, within the bound.
A program may use at most 64 MiB of HBM per device.

v0:
```python
import jax
import jax.numpy as jnp
from jax import lax
from jax.sharding import PartitionSpec as P

epsilon = 1e-06
masked_score = -1e30


def in_order(tiles, dim):
    shape = list(tiles.shape[1:])
    shape[dim] *= tiles.shape[0]
    return jnp.moveaxis(tiles, 0, dim).reshape(shape)


def sent_to_all(value, axis):
    count = lax.axis_size(axis)
    return lax.all_to_all(
        jnp.broadcast_to(value[None], (count, *value.shape)), axis, 0, 0, tiled=True
    )


def gather_directly(value, axis, dim):
    return in_order(sent_to_all(value, axis), dim)


def passed_along(block, axis, distance):
    devices = range(lax.axis_size(axis))
    route = [(i - distance, i) for i in devices if i - distance in devices]
    return lax.ppermute(block, axis, route)


def sent_together(arrays, axis, dim, along):
    ends, at = ([], 0)
    for a in arrays[:-1]:
        at += a.shape[along]
        ends.append(at)
    both = jnp.concatenate(arrays, axis=along)
    return tuple(jnp.split(lax.all_gather(both, axis, axis=dim, tiled=True), ends, axis=along))


def cut_along(value, dim, count):
    shape = value.shape
    tiles = value.reshape(*shape[:dim], count, shape[dim] // count, *shape[dim + 1 :])
    return jnp.moveaxis(tiles, dim, 0)


def sum_at_owner(value, axis, dim):
    tiles = cut_along(value, dim, lax.axis_size(axis))
    arrived = lax.all_to_all(tiles, axis, split_axis=0, concat_axis=0, tiled=True)
    return arrived.astype(jnp.float32).sum(axis=0)


def shards(
    tokens,
    norm_gain,
    w_query,
    w_key,
    w_value,
    w_conv_value,
    w_conv_pre,
    w_conv_post,
    conv_taps,
    log_gate_cache,
    w_out_conv,
    w_out_attn,
):
    float_rows = tokens.astype(jnp.float32)
    scaled = float_rows * lax.rsqrt(
        jnp.mean(float_rows * float_rows, axis=1, keepdims=True) + epsilon
    )
    normed_own = (scaled * norm_gain).astype(jnp.bfloat16)
    normed = gather_directly(normed_own, ("fs", "tp"), 0)
    block_rows = normed.shape[0]
    channels = w_conv_post.shape[1]
    head_dim = w_key.shape[1]
    local_heads = w_query.shape[1] // head_dim
    group = lax.axis_index(("fs", "tp"))
    local_weight = jnp.concatenate([w_conv_post, w_conv_pre, w_conv_value, w_query], axis=1)
    projected = jnp.dot(normed, local_weight, preferred_element_type=jnp.float32).astype(
        jnp.bfloat16
    )
    post_gate = projected[:, :channels]
    pre_gate = projected[:, channels : 2 * channels]
    conv_value = projected[:, 2 * channels : 3 * channels]
    queries = projected[:, 3 * channels :].reshape(block_rows, local_heads, head_dim)
    mixed_in = (pre_gate.astype(jnp.float32) * conv_value.astype(jnp.float32)).astype(jnp.bfloat16)
    kernel = conv_taps.shape[0]
    carried = passed_along(mixed_in[block_rows - (kernel - 1) :], "sp", 1)
    extended = jnp.concatenate([carried, mixed_in], axis=0).astype(jnp.float32)
    tap_weights = lax.dynamic_slice_in_dim(conv_taps, group * channels, channels, 1).astype(
        jnp.float32
    )
    conv_sum = tap_weights[0] * extended[0:block_rows]
    for offset in range(1, kernel):
        conv_sum = conv_sum + tap_weights[offset] * extended[offset : offset + block_rows]
    conv_out = (post_gate.astype(jnp.float32) * conv_sum).astype(jnp.bfloat16)
    core_index = lax.axis_index("tp")
    half_rows = block_rows // 2
    own_rows = lax.dynamic_slice_in_dim(normed, core_index * half_rows, half_rows, 0)
    pair_weight = jnp.concatenate([w_key, w_value], axis=1)
    pair_rows = jnp.dot(own_rows, pair_weight, preferred_element_type=jnp.float32).astype(
        jnp.bfloat16
    )
    key_half = pair_rows[:, :head_dim]
    value_half = pair_rows[:, head_dim:]
    head_gates = lax.dynamic_slice_in_dim(log_gate_cache, group * local_heads, local_heads, 0)
    anchor = lax.axis_index("sp") * block_rows
    gate_query = lax.dynamic_slice_in_dim(head_gates, anchor, block_rows, 1).T
    sequence_places = anchor + lax.iota(jnp.int32, block_rows)
    score_scale = head_dim ** (-0.5)

    def absorb(carried_state, key_block, value_block, sub_start):
        running_max, running_sum, weighted = carried_state
        sub_width = key_block.shape[0]
        scores = (
            jnp.einsum("qhd,kd->qhk", queries, key_block, preferred_element_type=jnp.float32)
            * score_scale
        )
        gate_keys = lax.dynamic_slice_in_dim(head_gates, sub_start, sub_width, 1)
        scores = scores + gate_query[:, :, None] - gate_keys[None, :, :]
        key_positions = sub_start + lax.iota(jnp.int32, sub_width)
        scores = jnp.where(
            sequence_places[:, None, None] >= key_positions[None, None, :], scores, masked_score
        )
        new_max = jnp.maximum(running_max, jnp.max(scores, axis=2))
        rescale = jnp.exp(running_max - new_max)
        weights = jnp.exp(scores - new_max[:, :, None])
        running_sum = running_sum * rescale + jnp.sum(weights, axis=2)
        weighted = weighted * rescale[:, :, None] + jnp.einsum(
            "qhk,kd->qhd",
            weights.astype(jnp.bfloat16),
            value_block,
            preferred_element_type=jnp.float32,
        )
        return (new_max, running_sum, weighted)

    initial = (
        jnp.full((block_rows, local_heads), masked_score, jnp.float32),
        jnp.zeros((block_rows, local_heads), jnp.float32),
        jnp.zeros((block_rows, local_heads, head_dim), jnp.float32),
    )
    key_piece, value_piece = sent_together((key_half, value_half), ("sp", "tp"), 0, 1)
    key_count = key_piece.shape[0]
    sub_width = 512

    def sweep_keys(current):

        def absorb_step(running, step_index):
            sub_start = step_index * sub_width
            key_block = lax.dynamic_slice_in_dim(key_piece, sub_start, sub_width, 0)
            value_block = lax.dynamic_slice_in_dim(value_piece, sub_start, sub_width, 0)
            return (absorb(running, key_block, value_block, sub_start), None)

        result, unused = lax.scan(
            absorb_step, current, jnp.arange(key_count // sub_width, dtype=jnp.int32)
        )
        return result

    def keep_state(current):
        return current

    running_max, running_sum, weighted = lax.cond(
        jnp.int32(0) <= anchor + block_rows - 1, sweep_keys, keep_state, initial
    )
    attn_out = (
        (weighted / running_sum[:, :, None])
        .astype(jnp.bfloat16)
        .reshape(block_rows, local_heads * head_dim)
    )
    mixed = sum_at_owner(
        (
            jnp.dot(conv_out, w_out_conv, preferred_element_type=jnp.float32)
            + jnp.dot(attn_out, w_out_attn, preferred_element_type=jnp.float32)
        ).astype(jnp.bfloat16),
        ("fs", "tp"),
        0,
    )
    return mixed.astype(jnp.bfloat16)


def solution(mesh):
    placed = (
        P(("sp", "fs", "tp"), None),
        P(),
        P(None, ("fs", "tp")),
        P(None, "fs"),
        P(None, "fs"),
        P(None, ("fs", "tp")),
        P(None, ("fs", "tp")),
        P(None, ("fs", "tp")),
        P(),
        P(),
        P(("fs", "tp"), None),
        P(("fs", "tp"), None),
    )
    return jax.shard_map(
        shards, mesh=mesh, in_specs=placed, out_specs=P(("sp", "fs", "tp"), None), check_vma=False
    )
```

profile of v0, /device:TPU:1, one launch (start us, length us, event | category | flops | bytes accessed | tf_op | source)
XLA Modules:
  0.0 338.9 jit_solution(1472676226842385966)
XLA Ops:
  9.8 10.3 %all-to-all-start = ((bf16[8,32,2048]{2,1,0:T(8,128)(2,1)}), bf16[8,32,2048]{2,1,0:T(8,128)(2,1)S(1)}, u32[]{:S(2)}, u32[]{:S(2)}) async-start(bf16[8,32,2048]{2,1,0:T(8,128)(2,1)} %broadcast_in_dim.45), calls=%async_computation | async-start | bytes 2097152 | tf_op jit(solution)/shard_map/all_to_all | solution.py:18
  20.1 15.0 %all-to-all-done = bf16[8,32,2048]{2,1,0:T(8,128)(2,1)S(1)} async-done(((bf16[8,32,2048]{2,1,0:T(8,128)(2,1)}), bf16[8,32,2048]{2,1,0:T(8,128)(2,1)S(1)}, u32[]{:S(2)}, u32[]{:S(2)}) %all-to-all-start) | async-done | bytes 1048608 | tf_op jit(solution)/shard_map/all_to_all | solution.py:18
  35.1 2.1 convolution_convert_fusion
  38.0 2.6 fusion.25
  42.7 1.8 fusion.39
  44.5 79.7 %all-gather.2.cloned.1.call-done = bf16[16384,256]{1,0:T(8,128)(2,1)} async-done(((bf16[128,256]{1,0:T(8,128)(2,1)}), bf16[16384,256]{1,0:T(8,128)(2,1)}) %all-gather.2.cloned.1.call-update) | async-done | bytes 8388624 | tf_op jit(solution)/shard_map/all_gather | solution.py:39
  124.2 185.2 %conditional.1 = (f32[256,2]{0,1:T(2,128)}, f32[256,2,128]{0,2,1:T(8,128)S(1)}) conditional(s32[]{:T(128)} %convert_element_type.57, () %tuple.19, (bf16[16384,256]{1,0:T(8,128)(2,1)}, bf16[256,640]{1,0:T(8,128)(2,1)S(1)}, f32[16,16384]{1,0:T(8,128)}, s32[]{:T(128)}, s32[]{:T(128)}, /*index=5*/s32[256]{0:T(256)S(1)}, f32[256,2]{0,1:T(2,128)S(1)}) %tuple.20), branch_computations={%region_1.0_spmd, %region_2.7_spmd} | conditional | flops 136908032 | bytes 23123452 | solution.py:163
  124.2 5.7 %fusion.49 = (bf16[16384,128]{1,0:T(8,128)(2,1)}, bf16[16384,128]{1,0:T(8,128)(2,1)}) fusion(bf16[16384,256]{1,0:T(8,128)(2,1)} %get-tuple-element.102), kind=kLoop, calls=%fused_computation.73 | loop fusion | bytes 16777216 | tf_op jit(solution)/shard_map/split | solution.py:39
  131.5 177.7 %while.18 = (s32[]{:T(128)}, f32[256,2]{0,1:T(2,128)S(1)}, f32[256,2]{0,1:T(2,128)}, f32[256,2,128]{2,0,1:T(8,128)S(1)}, s32[256]{0:T(256)S(1)}, /*index=5*/s32[...) while((s32[]{:T(128)}, f32[256,2]{0,1:T(2,128)S(1)}, ...), condition=%wide.region_6.6_spmd.clone, body=%wide.region_3.5_spmd.clone.sunk | while | flops 136907776 | bytes 4377827 | solution.py:155
  133.1 1.3 fusion.65
  138.0 1.3 fusion.65
  143.5 1.3 fusion.65
  149.1 1.3 fusion.65
  154.7 1.3 fusion.65
  160.3 1.3 fusion.65
  165.8 1.3 fusion.65
  171.4 1.3 fusion.65
  177.0 1.3 fusion.65
  182.6 1.3 fusion.65
  188.1 1.3 fusion.65
  193.7 1.3 fusion.65
  199.3 1.3 fusion.65
  204.8 1.3 fusion.65
  210.4 1.3 fusion.65
  216.0 1.3 fusion.65
  221.6 1.3 fusion.65
  227.1 1.3 fusion.65
  232.7 1.3 fusion.65
  238.3 1.3 fusion.65
  243.9 1.3 fusion.65
  310.1 2.0 fusion.24
  312.2 19.1 %all_to_all.10 = bf16[8,32,2048]{2,1,0:T(8,128)(2,1)S(1)} all-to-all(bf16[8,32,2048]{2,1,0:T(8,128)(2,1)S(1)} %bitcast.40), channel_id=1, replica_groups=mesh['sp'=64,'fs'=4,'tp'=2] {'fs','tp'}, dimensions={0} | all-to-all | bytes 2097152 | tf_op jit(solution)/shard_map/all_to_all | solution.py:50
  (332 shorter events, 135.7 us)
Async XLA Ops:
  6.5 303.6 %copy-start = (bf16[256,2048]{1,0:T(8,128)(2,1)S(1)}, bf16[256,2048]{1,0:T(8,128)(2,1)}, u32[]{:S(2)}) copy-start(bf16[256,2048]{1,0:T(8,128)(2,1)} %param.27) | copy-start | bytes 3145732
  6.5 31.4 %copy-start.2 = (bf16[2048,128]{1,0:T(8,128)(2,1)S(1)}, bf16[2048,128]{1,0:T(8,128)(2,1)}, u32[]{:S(2)}) copy-start(bf16[2048,128]{1,0:T(8,128)(2,1)} %param.21) | copy-start | bytes 1572868
  9.8 25.3 %all-to-all-start = ((bf16[8,32,2048]{2,1,0:T(8,128)(2,1)}), bf16[8,32,2048]{2,1,0:T(8,128)(2,1)S(1)}, u32[]{:S(2)}, u32[]{:S(2)}) async-start(bf16[8,32,2048]{2,1,0:T(8,128)(2,1)} %broadcast_in_dim.45), calls=%async_computation | async-start | bytes 2097152 | tf_op jit(solution)/shard_map/all_to_all | solution.py:18
  20.1 104.1 %all-gather.2.cloned.1.call-start = ((), (), s32[]{:S(2)}) async-start(), calls=%async_computation.2 | async-start | bytes 8454144 | tf_op jit(solution)/shard_map/all_gather | solution.py:39
  38.0 4.8 %copy-start.1 = (bf16[128,2048]{1,0:T(8,128)(2,1)S(1)}, bf16[128,2048]{1,0:T(8,128)(2,1)}, u32[]{:S(2)}) copy-start(bf16[128,2048]{1,0:T(8,128)(2,1)} %param.26) | copy-start | bytes 1572868
  40.6 2.1 collective-permute-start
Sparse Core Ops, SparseCore 0:
  37.4 86.7 all-gather.1
where the time goes:
time: 342 us; the launch traced here: 339 us
  waiting for transfers between devices  94.7 us (28%)
  matrix products  90.6 us (26%)
  other arithmetic  54.8 us (16%)
  local copies, waits for them, and re-layouts  30.5 us (9%)
  loops' own time  24.2 us (7%)
  blocking collectives  19.1 us (6%)
  between operations  13.5 us (4%)
  starting transfers between devices  11.6 us (3%)
    all_gather x1, waiting for transfers between devices, sent_together(): lax.all_gather(both, axis, axis=dim, tiled=True)  79.7 us
    dot_general x32, matrix products, absorb(): jnp.einsum('qhd,kd->qhk', queries, key_block, preferred_element_type=jnp....  41.6 us
    dot_general x32, matrix products, absorb(): jnp.einsum('qhk,kd->qhd', weights.astype(jnp.bfloat16), value_block, pref...  40.5 us
    add x32, other arithmetic, absorb(): running_sum = running_sum * rescale + jnp.sum(weights, axis=2)  40.3 us
    another operation x1, loops' own time, sweep_keys(): lax.scan(absorb_step, current, jnp.arange(key_count // sub_width, dtype=j...  24.2 us
    dynamic_slice x32, local copies, waits for them, and re-layouts, sweep_keys(): lax.scan(absorb_step, current, jnp.arange(key_count // sub_width, dtype=j...  20.8 us
    all_to_all x1, blocking collectives, sum_at_owner(): lax.all_to_all(tiles, axis, split_axis=0, concat_axis=0, tiled=True)  19.1 us
    all_to_all x1, waiting for transfers between devices, sent_to_all(): lax.all_to_all(jnp.broadcast_to(value[None], (count, *value.shape)), axis...  15 us
  transfers between devices with their start and end apart: 3, of which 2 were waited for; matrix products, arithmetic and copies ran while one was open for 2% of the time, Pallas kernels for 0%

commit v1 on v0

v1 whole, which is shorter than its diff:
```python
import functools
import math

import jax
import jax.numpy as jnp
from jax import lax
from jax.experimental import pallas as pl
from jax.experimental.pallas import tpu as pltpu
from jax.sharding import PartitionSpec as P

epsilon = 1e-06
masked_score = -1e30
MESH = pl.DeviceIdType.MESH
RING = 8


def in_order(tiles, dim):
    shape = list(tiles.shape[1:])
    shape[dim] *= tiles.shape[0]
    return jnp.moveaxis(tiles, 0, dim).reshape(shape)


def sent_to_all(value, axis):
    count = lax.axis_size(axis)
    return lax.all_to_all(
        jnp.broadcast_to(value[None], (count, *value.shape)), axis, 0, 0, tiled=True
    )


def gather_directly(value, axis, dim):
    return in_order(sent_to_all(value, axis), dim)


def passed_along(block, axis, distance):
    devices = range(lax.axis_size(axis))
    route = [(i - distance, i) for i in devices if i - distance in devices]
    return lax.ppermute(block, axis, route)


def cut_along(value, dim, count):
    shape = value.shape
    tiles = value.reshape(*shape[:dim], count, shape[dim] // count, *shape[dim + 1 :])
    return jnp.moveaxis(tiles, dim, 0)


def sum_at_owner(value, axis, dim):
    tiles = cut_along(value, dim, lax.axis_size(axis))
    arrived = lax.all_to_all(tiles, axis, split_axis=0, concat_axis=0, tiled=True)
    return arrived.astype(jnp.float32).sum(axis=0)


def attention_kernel(
    ring,
    q_ref,
    kv_ref,
    gate_ref,
    out_ref,
    own,
    other,
    row_max,
    row_sum,
    total,
    s1,
    sr,
    sl,
    sd,
    r_own,
    r_other,
):
    half = ring // 2
    sp = lax.axis_index("sp")
    core = lax.axis_index("tp")
    z, y = sp // ring, sp % ring
    far = 1 - core

    def first_axis(step):
        y1 = (y + far * step + ring) % ring
        z1 = (z + core * step + ring) % ring
        return {"sp": z1 * ring + y1}

    def second_axis(step):
        y1 = (y + core * step + ring) % ring
        z1 = (z + far * step + ring) % ring
        return {"sp": z1 * ring + y1}

    partner = {"tp": far}
    barrier = pltpu.get_barrier_semaphore()
    for who in (first_axis(1), first_axis(-1), second_axis(1), second_axis(-1), partner):
        pl.semaphore_signal(barrier, inc=1, device_id=who, device_id_type=MESH)
    own[0, 0] = kv_ref[...]
    row_max[...] = jnp.full_like(row_max, masked_score)
    row_sum[...] = jnp.zeros_like(row_sum)
    total[...] = jnp.zeros_like(total)
    pl.semaphore_wait(barrier, 5)

    def copy(src, dst, send, recv, who):
        return pltpu.make_async_remote_copy(
            src_ref=src, dst_ref=dst, send_sem=send, recv_sem=recv, device_id=who, device_id_type=MESH
        )

    def along(src, j, step):
        return copy(src, own.at[0, j], s1.at[j], r_own.at[0, j], first_axis(step))

    def right(src, slot, j):
        return copy(src, own.at[slot, j], sr.at[slot, j], r_own.at[slot, j], second_axis(1))

    def left(src, slot, j):
        return copy(src, own.at[slot, j], sl.at[slot, j], r_own.at[slot, j], second_axis(-1))

    def across(src, slot, j):
        return copy(src, other.at[slot, j], sd.at[slot, j], r_other.at[slot, j], partner)

    def arrived(slot, j):
        copy(own.at[slot, j], own.at[slot, j], sd.at[slot, j], r_own.at[slot, j], partner).wait_recv()

    def arrived_other(slot, j):
        copy(other.at[slot, j], other.at[slot, j], sd.at[slot, j], r_other.at[slot, j], partner).wait_recv()

    heads = 2
    rows = q_ref.shape[0] // heads
    depth = q_ref.shape[1]
    block = own.shape[3]
    group = ring // 2
    factor = depth ** (-0.5) * math.log2(math.e)

    def place(slot, j, origin):
        dp = slot - (slot // (half + 1)) * (2 * slot - half)
        ds = (j + 1) // 2 * (2 * (j % 2) - 1)
        z1 = (z - dp + origin * (dp - ds) + 2 * ring) % ring
        y1 = (y - ds + origin * (ds - dp) + 2 * ring) % ring
        return z1 * ring + y1

    def attend(buffer, slot, part, origin, diagonal=False):
        start = part * group
        keys = buffer[slot, pl.ds(start, group), 0].reshape(group * block, depth)
        values = buffer[slot, pl.ds(start, group), 1].reshape(group * block, depth)
        for head in range(heads):
            here = pl.ds(head * rows, rows)
            biases = []
            for i in range(group):
                from_sp = place(slot, start + i, origin)
                bias = jnp.where(from_sp <= sp, 0.0, masked_score).astype(jnp.float32)
                biases.append(gate_ref[head, pl.ds(from_sp * 2 + origin, 1), :] + bias)
            score = lax.dot_general(
                q_ref[here, :], keys, (((1,), (1,)), ((), ())), preferred_element_type=jnp.float32
            )
            score = score * factor + jnp.concatenate(biases, axis=1)
            if diagonal:
                at = lax.broadcasted_iota(jnp.int32, score.shape, 0)
                key = lax.broadcasted_iota(jnp.int32, score.shape, 1)
                hidden = (key < block) & (key + origin * block > at)
                score = jnp.where(hidden, masked_score, score)
            old = row_max[here, :]
            new = jnp.maximum(old, jnp.max(score, axis=1, keepdims=True))
            rescale = jnp.exp2(old - new)
            weight = jnp.exp2(score - jnp.concatenate([new] * (score.shape[1] // 128), axis=1))
            lanes = weight[:, :128]
            for i in range(1, score.shape[1] // 128):
                lanes = lanes + weight[:, i * 128 : (i + 1) * 128]
            row_max[here, :] = new
            row_sum[here, :] = row_sum[here, :] * rescale + lanes
            total[here, :] = total[here, :] * rescale + jnp.dot(
                weight.astype(jnp.bfloat16), values, preferred_element_type=jnp.float32
            )

    for j in range(ring):
        if j == 0:
            piece = kv_ref
            along(piece, 1, 1).start()
            along(piece, 2, -1).start()
        else:
            piece = own.at[0, j]
            arrived(0, j)
            if j + 2 < ring:
                along(piece, j + 2, 1 if j % 2 else -1).start()
        right(piece, 1, j).start()
        left(piece, half + 1, j).start()
        across(piece, 0, j).start()

    for hop in range(1, half):
        r, l = hop, half + hop

        def pass_on(j, odd):
            arrived(r, j)
            if hop < half - 1:
                right(own.at[r, j], r + 1, j).start()
            elif odd:
                right(own.at[r, j], half, j).start()
            across(own.at[r, j], r, j).start()
            arrived(l, j)
            if hop < half - 1:
                left(own.at[l, j], l + 1, j).start()
            elif not odd:
                left(own.at[l, j], half, j).start()
            across(own.at[l, j], l, j).start()

        if hop == 1:

            def wait_other(slot, part):
                for i in range(group):
                    arrived_other(slot, part * group + i)

            for quarter in range(4):
                for i in range(ring // 4):
                    j = quarter * (ring // 4) + i
                    pass_on(j, j % 2)
                if quarter < 2:
                    attend(own, 0, quarter, core, diagonal=quarter == 0)
                else:
                    wait_other(0, quarter - 2)
                    attend(other, 0, quarter - 2, far, diagonal=quarter == 2)
        else:

            def step(t, carry):
                slot = r - 1 + (t // 2) * half
                part = t % 2
                for i in range(ring // 8):
                    pass_on(2 * t, 0)
                attend(own, slot, part, core)
                for i in range(ring // 8):
                    pass_on(2 * t + 1, 1)
                for i in range(group):
                    arrived_other(slot, part * group + i)
                attend(other, slot, part, far)
                return carry

            lax.fori_loop(0, 4, step, 0)

    def last(t, carry):
        slot = half - 1 + (t // 2) * half
        part = t % 2
        for i in range(2):
            arrived(half, 2 * t + i)
            across(own.at[half, 2 * t + i], half, 2 * t + i).start()
        attend(own, slot, part, core)
        for i in range(group):
            arrived_other(slot, part * group + i)
        attend(other, slot, part, far)
        return carry

    lax.fori_loop(0, 4, last, 0)

    def tail(t, carry):
        attend(own, half, t, core)
        for i in range(group):
            arrived_other(half, t * group + i)
        attend(other, half, t, far)
        return carry

    lax.fori_loop(0, 2, tail, 0)

    for head in range(heads):
        here = pl.ds(head * rows, rows)
        out_ref[:, pl.ds(head * depth, depth)] = (
            total[here, :] / jnp.sum(row_sum[here, :], axis=1, keepdims=True)
        ).astype(out_ref.dtype)

    for j in range(1, ring):
        along(own.at[0, j], j, 1).wait_send()

    def sent(j, carry):
        for slot in range(1, half):
            right(own.at[slot, j], slot, j).wait_send()
            left(own.at[half + slot, j], half + slot, j).wait_send()
        for slot in range(ring):
            across(own.at[slot, j], slot, j).wait_send()
        return carry

    lax.fori_loop(0, ring, sent, 0)

    def sent_far(t, carry):
        right(own.at[half, 2 * t + 1], half, 2 * t + 1).wait_send()
        left(own.at[half, 2 * t], half, 2 * t).wait_send()
        return carry

    lax.fori_loop(0, half, sent_far, 0)


def attention(q, kv, gates, ring):
    rows, depth = q.shape
    block = kv.shape[1]
    slots = pltpu.VMEM((ring, ring, 2, block, depth), kv.dtype)
    dma = pltpu.SemaphoreType.DMA
    return pl.pallas_call(
        functools.partial(attention_kernel, ring),
        out_shape=jax.ShapeDtypeStruct((rows // 2, 2 * depth), jnp.bfloat16),
        in_specs=[pl.BlockSpec(memory_space=pltpu.VMEM)] * 3,
        out_specs=pl.BlockSpec(memory_space=pltpu.VMEM),
        scratch_shapes=[
            slots,
            slots,
            pltpu.VMEM((rows, 128), jnp.float32),
            pltpu.VMEM((rows, 128), jnp.float32),
            pltpu.VMEM((rows, depth), jnp.float32),
            dma((ring,)),
            dma((ring, ring)),
            dma((ring, ring)),
            dma((ring, ring)),
            dma((ring, ring)),
            dma((ring, ring)),
        ],
        compiler_params=pltpu.CompilerParams(
            collective_id=0, has_side_effects=True, vmem_limit_bytes=48 << 20
        ),
        cost_estimate=pl.CostEstimate(
            flops=4 * rows * depth * block * 2 * ring * ring, bytes_accessed=1 << 22, transcendentals=0
        ),
        name="gather_attend",
    )(q, kv, gates)


def shards(
    tokens,
    norm_gain,
    w_query,
    w_key,
    w_value,
    w_conv_value,
    w_conv_pre,
    w_conv_post,
    conv_taps,
    log_gate_cache,
    w_out_conv,
    w_out_attn,
):
    float_rows = tokens.astype(jnp.float32)
    scaled = float_rows * lax.rsqrt(
        jnp.mean(float_rows * float_rows, axis=1, keepdims=True) + epsilon
    )
    normed_own = (scaled * norm_gain).astype(jnp.bfloat16)
    normed = gather_directly(normed_own, ("fs", "tp"), 0)
    block_rows = normed.shape[0]
    channels = w_conv_post.shape[1]
    head_dim = w_key.shape[1]
    local_heads = w_query.shape[1] // head_dim
    group = lax.axis_index(("fs", "tp"))
    core_index = lax.axis_index("tp")
    half_rows = block_rows // 2
    own_rows = lax.dynamic_slice_in_dim(normed, core_index * half_rows, half_rows, 0)
    kv = jnp.stack(
        [
            jnp.dot(own_rows, w, preferred_element_type=jnp.float32).astype(jnp.bfloat16)
            for w in (w_key, w_value)
        ]
    )
    queries = jnp.dot(normed, w_query, preferred_element_type=jnp.float32).astype(jnp.bfloat16)
    queries = jnp.moveaxis(queries.reshape(block_rows, local_heads, head_dim), 1, 0)
    head_gates = lax.dynamic_slice_in_dim(log_gate_cache, group * local_heads, local_heads, 0)
    gates = (head_gates * (-math.log2(math.e))).reshape(local_heads, -1, half_rows)
    ring = math.isqrt(lax.axis_size("sp"))
    attn_out = attention(queries.reshape(local_heads * block_rows, head_dim), kv, gates, ring)

    local_weight = jnp.concatenate([w_conv_post, w_conv_pre, w_conv_value], axis=1)
    projected = jnp.dot(normed, local_weight, preferred_element_type=jnp.float32).astype(
        jnp.bfloat16
    )
    post_gate = projected[:, :channels]
    pre_gate = projected[:, channels : 2 * channels]
    conv_value = projected[:, 2 * channels : 3 * channels]
    mixed_in = (pre_gate.astype(jnp.float32) * conv_value.astype(jnp.float32)).astype(jnp.bfloat16)
    kernel = conv_taps.shape[0]
    carried = passed_along(mixed_in[block_rows - (kernel - 1) :], "sp", 1)
    extended = jnp.concatenate([carried, mixed_in], axis=0).astype(jnp.float32)
    tap_weights = lax.dynamic_slice_in_dim(conv_taps, group * channels, channels, 1).astype(
        jnp.float32
    )
    conv_sum = tap_weights[0] * extended[0:block_rows]
    for offset in range(1, kernel):
        conv_sum = conv_sum + tap_weights[offset] * extended[offset : offset + block_rows]
    conv_out = (post_gate.astype(jnp.float32) * conv_sum).astype(jnp.bfloat16)

    mixed = sum_at_owner(
        (
            jnp.dot(conv_out, w_out_conv, preferred_element_type=jnp.float32)
            + jnp.dot(attn_out, w_out_attn, preferred_element_type=jnp.float32)
        ).astype(jnp.bfloat16),
        ("fs", "tp"),
        0,
    )
    return mixed.astype(jnp.bfloat16)


def solution(mesh):
    placed = (
        P(("sp", "fs", "tp"), None),
        P(),
        P(None, ("fs", "tp")),
        P(None, "fs"),
        P(None, "fs"),
        P(None, ("fs", "tp")),
        P(None, ("fs", "tp")),
        P(None, ("fs", "tp")),
        P(),
        P(),
        P(("fs", "tp"), None),
        P(("fs", "tp"), None),
    )
    return jax.shard_map(
        shards, mesh=mesh, in_specs=placed, out_specs=P(("sp", "fs", "tp"), None), check_vma=False
    )
```

time: 342 us -> 112 us (0.33)
  matrix products: 90.6 us -> 6.14 us
  waiting for transfers between devices: 94.7 us -> 13.2 us
  Pallas kernels: 0 us -> 54.9 us
  other arithmetic: 54.8 us -> 4.81 us
  local copies, waits for them, and re-layouts: 30.5 us -> 1.25 us
  loops' own time: 24.2 us -> 0 us
  between operations: 13.5 us -> 0.14 us
    dot_general x65 -> x3, matrix products: 84.2 us -> 3.18 us  [the longest x2 2.66 us: shards(): jnp.dot(own_rows, w, preferred_element_type=jnp.float32)]
    all_gather x1 -> x0, waiting for transfers between devices: 79.7 us -> none  [sent_together(): lax.all_gather(both, axis, axis=dim, tiled=True)]
    pallas_call x0 -> x1, Pallas kernels: none -> 54.9 us  [attention(): pl.pallas_call(functools.partial(attention_kernel, ring), out_shape=jax.S...]
    add x65 -> x0, other arithmetic: 40.5 us -> none  [the longest x32 40.3 us: absorb(): running_sum = running_sum * rescale + jnp.sum(weights, axis=2)]
    another operation x2 -> x0, loops' own time: 24.2 us -> none  [the longest x1 24.2 us: sweep_keys(): lax.scan(absorb_step, current, jnp.arange(key_count // sub_width, dtype=j...]
    dynamic_slice x65 -> x0, local copies, waits for them, and re-layouts: 22.3 us -> none  [the longest x32 20.8 us: sweep_keys(): lax.scan(absorb_step, current, jnp.arange(key_count // sub_width, dtype=j...]
    split x1 -> x0, local copies, waits for them, and re-layouts: 5.68 us -> none  [sent_together(): jnp.split(lax.all_gather(both, axis, axis=dim, tiled=True), ends, axis=al...]
    reduce_sum x32 -> x0, other arithmetic: 5.17 us -> none  [absorb(): running_sum = running_sum * rescale + jnp.sum(weights, axis=2)]
  transfers between devices with their start and end apart: 3 -> 2, of which waited for: 2 -> 1; matrix products, arithmetic and copies ran while one was open for 2% -> 2% of each run, Pallas kernels for 0% -> 49%
where the time goes in v1:
time: 112 us
  Pallas kernels  54.9 us (49%)
  blocking collectives  19.8 us (18%)
  waiting for transfers between devices  13.2 us (12%)
  starting transfers between devices  11.7 us (10%)
  matrix products  6.14 us (5%)
  other arithmetic  4.81 us (4%)
  local copies, waits for them, and re-layouts  1.25 us (1%)
    pallas_call x1, Pallas kernels, attention(): pl.pallas_call(functools.partial(attention_kernel, ring), out_shape=jax.S...  54.9 us
    all_to_all x1, blocking collectives, sum_at_owner(): lax.all_to_all(tiles, axis, split_axis=0, concat_axis=0, tiled=True)  19.8 us
    all_to_all x1, waiting for transfers between devices, sent_to_all(): lax.all_to_all(jnp.broadcast_to(value[None], (count, *value.shape)), axis...  13.2 us
    all_to_all x1, starting transfers between devices, sent_to_all(): lax.all_to_all(jnp.broadcast_to(value[None], (count, *value.shape)), axis...  10.4 us
    dot_general x2, matrix products, shards(): jnp.dot(own_rows, w, preferred_element_type=jnp.float32)  2.66 us
  transfers between devices with their start and end apart: 2, of which 1 were waited for; matrix products, arithmetic and copies ran while one was open for 2% of the time, Pallas kernels for 49%

profile of v1, /device:TPU:1, one launch (start us, length us, event | category | flops | bytes accessed | tf_op | source)
XLA Modules:
  0.0 111.9 jit_solution(16635406538143272260)
XLA Ops:
  0.0 0.0 copy-start
  0.0 1.1 %fusion.14 = f32[32]{0:T(128)S(1)} fusion(bf16[32,2048]{1,0:T(8,128)(2,1)} %param.12), kind=kLoop, calls=%fused_computation.18 | loop fusion | flops 196576 | bytes 131200 | tf_op jit(solution)/shard_map/reduce_sum | solution.py:328
  1.1 1.0 fusion.16
  2.2 1.1 broadcast_in_dim.2
  3.3 0.0 copy-start.1
  3.3 10.4 %all-to-all-start = ((bf16[8,32,2048]{2,1,0:T(8,128)(2,1)}), bf16[8,32,2048]{2,1,0:T(8,128)(2,1)S(1)}, u32[]{:S(2)}, u32[]{:S(2)}) async-start(bf16[8,32,2048]{2,1,0:T(8,128)(2,1)} %broadcast_in_dim.2), calls=%async_computation | async-start | bytes 2097152 | tf_op jit(solution)/shard_map/all_to_all | solution.py:25
  13.7 1.1 multiply_bitcast_fusion
  14.8 0.7 dynamic-slice_convert_fusion
  15.5 13.2 %all-to-all-done = bf16[8,32,2048]{2,1,0:T(8,128)(2,1)S(1)} async-done(((bf16[8,32,2048]{2,1,0:T(8,128)(2,1)}), bf16[8,32,2048]{2,1,0:T(8,128)(2,1)S(1)}, u32[]{:S(2)}, u32[]{:S(2)}) %all-to-all-start) | async-done | bytes 1048608 | tf_op jit(solution)/shard_map/all_to_all | solution.py:25
  28.7 1.3 %fusion.11 = bf16[1,128,128]{2,1,0:T(8,128)(2,1)S(1)} fusion(bf16[2048,128]{1,0:T(8,128)(2,1)} %param.16, bf16[256,2048]{1,0:T(8,128)(2,1)S(1)} %bitcast.31, s32[]{:T(128)S(6)} %select_n.10), kind=kOutput, calls=%fused_computation.13 | convolution fusion | flops 67125248 | bytes 1081348 | tf_op jit(solution)/shard_map/dot_general | solution.py:342
  30.0 1.3 %fusion.10 = bf16[1,128,128]{2,1,0:T(8,128)(2,1)S(1)} fusion(bf16[2048,128]{1,0:T(8,128)(2,1)} %param.15, bf16[256,2048]{1,0:T(8,128)(2,1)S(1)} %bitcast.32, s32[]{:T(128)S(6)} %select_n.10), kind=kOutput, calls=%fused_computation.12 | convolution fusion | flops 67125248 | bytes 1081348 | tf_op jit(solution)/shard_map/dot_general | solution.py:342
  31.4 0.0 copy-done.1
  31.4 0.5 convolution_convert_fusion
  31.9 0.1 copy.13
  32.0 2.1 %fusion.7 = bf16[256,384]{1,0:T(8,128)(2,1)S(1)} fusion(bf16[256,2048]{1,0:T(8,128)(2,1)S(1)} %bitcast.34, bf16[2048,128]{1,0:T(8,128)(2,1)} %param.17, bf16[2048,128]{1,0:T(8,128)(2,1)} %param.18, bf16[2048,128]{1,0:T(8,128)(2,1)} %param.19), kind=kOutput, calls=%fused_computation.8 | convolution fusion | flops 407470080 | bytes 2818048 | tf_op jit(solution)/shard_map/dot_general | solution.py:354
  34.1 1.3 %collective-permute-start = (bf16[2,128]{1,0:T(2,128)(2,1)S(1)}, bf16[2,128]{1,0:T(2,128)(2,1)S(1)}, u32[]{:S(2)}, u32[]{:S(2)}) collective-permute-start(bf16[2,128]{1,0:T(2,128)(2,1)S(1)} %slice.43), channel_id=1, source_target_pairs={{0,8},{8,16},{16,24},{24,32},{32,40},{40,48},{48,56},{56,64},{64,7... | collective-permute-start | bytes 1544 | tf_op jit(solution)/shard_map/ppermute | solution.py:37
  35.4 0.0 copy-start.2
  35.4 54.9 %gather_attend.1 = bf16[256,256]{1,0:T(8,128)(2,1)S(1)} custom-call(bf16[512,128]{1,0:T(8,128)(2,1)S(1)} %bitcast.30, bf16[2,128,128]{2,1,0:T(8,128)(2,1)S(1)} %pad_maximum_fusion.kv_ref, f32[2,128,128]{2,1,0:T(8,128)S(1)} %bitcast.29), custom_call_target="tpu_custom_call" | custom-call | flops 4294967296 | bytes 4194304 | tf_op jit(solution)/shard_map/gather_attend/pallas_call | solution.py:284
  90.3 0.0 collective-permute-done
  90.4 0.0 copy-done.2
  90.4 0.4 fusion.21
  90.8 0.0 copy-done
  90.8 0.5 fusion
  91.3 19.8 %all_to_all.10 = bf16[8,32,2048]{2,1,0:T(8,128)(2,1)S(1)} all-to-all(bf16[8,32,2048]{2,1,0:T(8,128)(2,1)S(1)} %bitcast.35), channel_id=1, replica_groups=mesh['sp'=64,'fs'=4,'tp'=2] {'fs','tp'}, dimensions={0} | all-to-all | bytes 2097152 | tf_op jit(solution)/shard_map/all_to_all | solution.py:48
  111.1 0.8 reduce_sum.22
  (7 shorter events, 0.1 us)
Async XLA Ops:
  0.0 90.8 %copy-start = (bf16[256,2048]{1,0:T(8,128)(2,1)S(1)}, bf16[256,2048]{1,0:T(8,128)(2,1)}, u32[]{:S(2)}) copy-start(bf16[256,2048]{1,0:T(8,128)(2,1)} %param.23) | copy-start | bytes 3145732
  3.3 28.1 %copy-start.1 = (bf16[2048,256]{1,0:T(8,128)(2,1)S(1)}, bf16[2048,256]{1,0:T(8,128)(2,1)}, u32[]{:S(2)}) copy-start(bf16[2048,256]{1,0:T(8,128)(2,1)} %param.14) | copy-start | bytes 3145732
  3.3 25.4 %all-to-all-start = ((bf16[8,32,2048]{2,1,0:T(8,128)(2,1)}), bf16[8,32,2048]{2,1,0:T(8,128)(2,1)S(1)}, u32[]{:S(2)}, u32[]{:S(2)}) async-start(bf16[8,32,2048]{2,1,0:T(8,128)(2,1)} %broadcast_in_dim.2), calls=%async_computation | async-start | bytes 2097152 | tf_op jit(solution)/shard_map/all_to_all | solution.py:25
  34.1 56.2 %collective-permute-start = (bf16[2,128]{1,0:T(2,128)(2,1)S(1)}, bf16[2,128]{1,0:T(2,128)(2,1)S(1)}, u32[]{:S(2)}, u32[]{:S(2)}) collective-permute-start(bf16[2,128]{1,0:T(2,128)(2,1)S(1)} %slice.43), channel_id=1, source_target_pairs={{0,8},{8,16},{16,24},{24,32},{32,40},{40,48},{48,56},{56,64},{64,7... | collective-permute-start | bytes 1544 | tf_op jit(solution)/shard_map/ppermute | solution.py:37
  35.4 54.9 %copy-start.2 = (bf16[128,2048]{1,0:T(8,128)(2,1)S(1)}, bf16[128,2048]{1,0:T(8,128)(2,1)}, u32[]{:S(2)}) copy-start(bf16[128,2048]{1,0:T(8,128)(2,1)} %param.22) | copy-start | bytes 1572868

commit v2 on v1

v2 whole, which is shorter than its diff:
```python
import functools
import math

import jax
import jax.numpy as jnp
from jax import lax
from jax.experimental import pallas as pl
from jax.experimental.pallas import tpu as pltpu
from jax.sharding import PartitionSpec as P

epsilon = 1e-06
masked_score = -1e30
MESH = pl.DeviceIdType.MESH
log2_e = math.log2(math.e)


def arrival_order(ring):
    half = ring // 2
    pieces = []
    for slot in range(ring):
        hops = slot if slot <= half else slot - half
        for j in range(ring):
            pieces.append((hops + (j + 1) // 2, hops, slot, j))
    return [(slot, j) for _, _, slot, j in sorted(pieces)]


def chosen(values, t):
    if isinstance(t, int):
        return values[t]
    words = [values[n : n + 8] for n in range(0, len(values), 8)]
    packed = [sum(v << (3 * n) for n, v in enumerate(word)) for word in words]
    picked = jnp.int32(packed[-1])
    for n in range(len(packed) - 2, -1, -1):
        picked = jnp.where(t < 8 * (n + 1), jnp.int32(packed[n]), picked)
    return (picked >> (3 * (t % 8))) & 7


def layer_kernel(
    ring,
    tokens,
    gain,
    w_query,
    w_key,
    w_value,
    w_conv_value,
    w_conv_pre,
    w_conv_post,
    taps,
    log_gates,
    w_out_conv,
    w_out_attn,
    out_ref,
    rows,
    wq,
    wkv,
    wconv,
    wout,
    gates,
    bias_of,
    q_ref,
    own,
    other,
    row_max,
    row_sum,
    total,
    mixed_tail,
    halo,
    extended,
    gate_after,
    merged,
    part_keep,
    part_send,
    part_come,
    pair,
    relay,
    passed,
    come,
    weight_sem,
    gx_send,
    gx_recv,
    gd_send,
    gd_recv,
    halo_sem,
    s1,
    sr,
    sl,
    sd,
    r_own,
    r_other,
    pd_send,
    pd_recv,
    relay_send,
    relay_recv,
    come_send,
    come_recv,
):
    half = ring // 2
    group = ring // 2
    sp = lax.axis_index("sp")
    x = lax.axis_index("fs")
    core = lax.axis_index("tp")
    z, y = sp // ring, sp % ring
    far = 1 - core
    device = x * 2 + core
    blocks = ring * ring
    bf16 = jnp.bfloat16
    f32 = jnp.float32

    def first_axis(step):
        y1 = (y + far * step + ring) % ring
        z1 = (z + core * step + ring) % ring
        return {"sp": z1 * ring + y1}

    def second_axis(step):
        y1 = (y + core * step + ring) % ring
        z1 = (z + far * step + ring) % ring
        return {"sp": z1 * ring + y1}

    def along_x(step):
        return {"fs": (x + step + 4) % 4}

    partner = {"tp": far}
    after = {"sp": (sp + 1) % blocks}
    before = {"sp": (sp + blocks - 1) % blocks}

    def copy(src, dst, send, recv, who):
        return pltpu.make_async_remote_copy(
            src_ref=src, dst_ref=dst, send_sem=send, recv_sem=recv, device_id=who, device_id_type=MESH
        )

    depth = w_key.shape[1]
    channels = w_conv_post.shape[1]
    loads = [
        (log_gates, gates),
        (w_key, wkv.at[:, pl.ds(0, depth)]),
        (w_value, wkv.at[:, pl.ds(depth, depth)]),
        (w_query, wq),
        (w_conv_post, wconv.at[:, pl.ds(0, channels)]),
        (w_conv_pre, wconv.at[:, pl.ds(channels, channels)]),
        (w_conv_value, wconv.at[:, pl.ds(2 * channels, channels)]),
        (w_out_conv, wout.at[pl.ds(0, channels)]),
        (w_out_attn, wout.at[pl.ds(channels, 2 * depth)]),
    ]
    loads = [pltpu.make_async_copy(a, b, weight_sem.at[n]) for n, (a, b) in enumerate(loads)]
    for load in loads:
        load.start()

    barrier = pltpu.get_barrier_semaphore()
    near = (
        first_axis(1),
        first_axis(-1),
        second_axis(1),
        second_axis(-1),
        partner,
        along_x(1),
        along_x(-1),
        after,
        before,
    )
    for who in near:
        pl.semaphore_signal(barrier, inc=1, device_id=who, device_id_type=MESH)

    wide = tokens[...].astype(f32)
    scaled = wide * lax.rsqrt(jnp.mean(wide * wide, axis=1, keepdims=True) + epsilon)
    rows[device] = (scaled * gain[...]).astype(bf16)
    row_max[...] = jnp.full_like(row_max, masked_score)
    row_sum[...] = jnp.zeros_like(row_sum)
    total[...] = jnp.zeros_like(total)
    pl.semaphore_wait(barrier, len(near))

    few = rows.shape[1] // 2

    def of_x(step):
        return (x + step + 4) % 4 * 2 + core

    def piece_of(step, h):
        return rows.at[of_x(step), pl.ds(h * few, few)]

    def gather_x(step, h, sem, way):
        return copy(piece_of(step, h), piece_of(step, h), gx_send.at[sem], gx_recv.at[sem], along_x(way))

    def gather_across(step, n):
        here = rows.at[of_x(step)]
        return copy(here, here, gd_send.at[n], gd_recv.at[n], partner)

    def came_x(step, h, sem):
        return copy(piece_of(step, h), piece_of(step, h), gx_send.at[sem], gx_recv.at[sem], partner)

    first = [
        gather_x(0, 0, 0, 1),
        gather_x(0, 1, 1, -1),
        gather_x(0, 1, 2, 1),
        gather_x(0, 0, 3, -1),
    ]
    for one in first:
        one.start()
    crossing = [gather_across(0, 0)]
    crossing[0].start()

    heads = 2
    keys_of_block = bias_of.shape[2]
    loads[0].wait()
    row = lax.broadcasted_iota(jnp.int32, (gates.shape[0], keys_of_block), 0)
    for head in range(heads):
        mine = row == device * heads + head
        for n in range(0, bias_of.shape[1], 8):
            lines = [
                jnp.sum(
                    jnp.where(mine, gates[:, b * keys_of_block : (b + 1) * keys_of_block], 0.0),
                    axis=0,
                    keepdims=True,
                )
                for b in range(n, n + 8)
            ]
            seen = n + lax.broadcasted_iota(jnp.int32, (8, keys_of_block), 0) < 2 * sp + 2
            bias_of[head, n : n + 8] = jnp.where(
                seen, jnp.concatenate(lines, axis=0) * -log2_e, masked_score
            )

    came_x(-1, 0, 0).wait_recv()
    second = [gather_x(-1, 0, 4, 1)]
    second[0].start()
    came_x(1, 1, 1).wait_recv()
    second.append(gather_x(1, 1, 5, -1))
    second[1].start()
    came_x(-1, 1, 2).wait_recv()
    crossing.append(gather_across(-1, 1))
    crossing[1].start()
    came_x(1, 0, 3).wait_recv()
    crossing.append(gather_across(1, 2))
    crossing[2].start()
    came_x(2, 0, 4).wait_recv()
    came_x(2, 1, 5).wait_recv()
    crossing.append(gather_across(2, 3))
    crossing[3].start()
    for n in range(4):
        here = rows.at[(x + (0, -1, 1, 2)[n] + 4) % 4 * 2 + far]
        copy(here, here, gd_send.at[n], gd_recv.at[n], partner).wait_recv()

    width = rows.shape[2]
    block = own.shape[3]
    loads[1].wait()
    loads[2].wait()
    half_rows = rows[pl.ds(4 * core, 4)].reshape(block, width)
    made = jnp.dot(half_rows, wkv[...], preferred_element_type=f32).astype(bf16)
    own[0, 0, 0] = made[:, :depth]
    own[0, 0, 1] = made[:, depth:]

    def along(src, j, step):
        return copy(src, own.at[0, j], s1.at[j], r_own.at[0, j], first_axis(step))

    def right(src, slot, j):
        return copy(src, own.at[slot, j], sr.at[slot, j], r_own.at[slot, j], second_axis(1))

    def left(src, slot, j):
        return copy(src, own.at[slot, j], sl.at[slot, j], r_own.at[slot, j], second_axis(-1))

    def across(src, slot, j):
        return copy(src, other.at[slot, j], sd.at[slot, j], r_other.at[slot, j], partner)

    def arrived(slot, j):
        copy(own.at[slot, j], own.at[slot, j], sd.at[slot, j], r_own.at[slot, j], partner).wait_recv()

    def arrived_other(slot, j):
        copy(other.at[slot, j], other.at[slot, j], sd.at[slot, j], r_other.at[slot, j], partner).wait_recv()

    here = own.at[0, 0]
    along(here, 1, 1).start()
    along(here, 2, -1).start()
    right(here, 1, 0).start()
    left(here, half + 1, 0).start()
    across(here, 0, 0).start()

    span = rows.shape[0] * rows.shape[1]
    all_rows = rows[...].reshape(span, width)
    loads[3].wait()
    asked = jnp.dot(all_rows, wq[...], preferred_element_type=f32).astype(bf16)
    for head in range(heads):
        q_ref[pl.ds(head * span, span), :] = asked[:, head * depth : (head + 1) * depth]
    for n in (4, 5, 6):
        loads[n].wait()
    projected = jnp.dot(all_rows, wconv[...], preferred_element_type=f32).astype(bf16)
    gate_after[...] = projected[:, :channels]
    mixed_in = (
        projected[:, channels : 2 * channels].astype(f32) * projected[:, 2 * channels :].astype(f32)
    ).astype(bf16)
    edge = halo.shape[0]
    mixed_tail[...] = mixed_in[span - edge :]
    extended[pl.ds(edge, span), :] = mixed_in.astype(f32)
    shift = copy(mixed_tail, halo, halo_sem.at[0], halo_sem.at[1], after)
    shift.start()
    factor = depth ** (-0.5) * log2_e

    def place(slot, j, origin):
        dp = slot - (slot // (half + 1)) * (2 * slot - half)
        ds = (j + 1) // 2 * (2 * (j % 2) - 1)
        z1 = (z - dp + origin * (dp - ds) + 2 * ring) % ring
        y1 = (y - ds + origin * (ds - dp) + 2 * ring) % ring
        return z1 * ring + y1

    def attend(buffer, pieces, origin, diagonal=False):
        keys = jnp.concatenate([buffer[slot, j, 0] for slot, j in pieces], axis=0)
        values = jnp.concatenate([buffer[slot, j, 1] for slot, j in pieces], axis=0)
        for head in range(heads):
            here = pl.ds(head * span, span)
            biases = []
            for slot, j in pieces:
                biases.append(bias_of[head, pl.ds(place(slot, j, origin) * 2 + origin, 1), :])
            score = lax.dot_general(
                q_ref[here, :], keys, (((1,), (1,)), ((), ())), preferred_element_type=f32
            )
            score = score * factor + jnp.concatenate(biases, axis=1)
            if diagonal:
                at = lax.broadcasted_iota(jnp.int32, score.shape, 0)
                key = lax.broadcasted_iota(jnp.int32, score.shape, 1)
                hidden = (key < block) & (key + origin * block > at)
                score = jnp.where(hidden, masked_score, score)
            old = row_max[here, :]
            new = jnp.maximum(old, jnp.max(score, axis=1, keepdims=True))
            rescale = jnp.exp2(old - new)
            weight = jnp.exp2(score - jnp.concatenate([new] * (score.shape[1] // 128), axis=1))
            lanes = weight[:, :128]
            for i in range(1, score.shape[1] // 128):
                lanes = lanes + weight[:, i * 128 : (i + 1) * 128]
            row_max[here, :] = new
            row_sum[here, :] = row_sum[here, :] * rescale + lanes
            total[here, :] = total[here, :] * rescale + jnp.dot(
                weight.astype(bf16), values, preferred_element_type=f32
            )

    order = arrival_order(ring)
    turns = len(order) // group

    def at_turn(t, i):
        slots = [order[n * group + i][0] for n in range(turns)]
        places = [order[n * group + i][1] for n in range(turns)]
        return chosen(slots, t), chosen(places, t)

    def pass_on(t):
        for i in range(group):
            slot, j = at_turn(t, i)
            here = own.at[slot, j]
            arrived(slot, j)
            odd = j % 2

            @pl.when((slot == 0) & (j + 2 < ring))
            def _():
                along(here, j + 2, 2 * odd - 1).start()

            @pl.when((slot < half - 1) | ((slot == half - 1) & (odd == 1)))
            def _():
                right(here, slot + 1, j).start()

            down = jnp.where(slot == 0, half, slot)

            @pl.when((slot == 0) | ((slot > half) & ((slot < ring - 1) | (odd == 0))))
            def _():
                left(here, jnp.where(slot == ring - 1, half, down + 1), j).start()

            across(here, slot, j).start()

    def attend_turn(t, diagonal=False):
        pieces = [at_turn(t, i) for i in range(group)]
        attend(own, pieces, core, diagonal)
        for slot, j in pieces:
            arrived_other(slot, j)
        attend(other, pieces, far, diagonal)

    for i in range(1, group):
        slot, j = order[i]
        here = own.at[slot, j]
        arrived(slot, j)
        if slot == 0:
            along(here, j + 2, 2 * (j % 2) - 1).start()
            left(here, half + 1, j).start()
        if slot > half:
            left(here, slot + 1, j).start()
        else:
            right(here, slot + 1, j).start()
        across(here, slot, j).start()
    pass_on(jnp.int32(1))
    attend_turn(0, diagonal=True)

    def turn(t, carry):
        pass_on(t)
        attend_turn(t - 1)
        return carry

    lax.fori_loop(2, turns, turn, 0)

    shift.wait()
    extended[pl.ds(0, edge), :] = jnp.where(sp == 0, 0.0, halo[...].astype(f32))
    at = pl.multiple_of(device * channels, channels)
    tap_rows = taps[:, pl.ds(at, channels)].astype(f32)
    count = tap_rows.shape[0]
    conv_sum = tap_rows[0:1] * extended[pl.ds(edge - count + 1, span), :]
    for n in range(1, count):
        conv_sum = conv_sum + tap_rows[n : n + 1] * extended[pl.ds(edge - count + 1 + n, span), :]
    merged[:, pl.ds(0, channels)] = (gate_after[...].astype(f32) * conv_sum).astype(bf16)

    attend_turn(turns - 1)
    for head in range(heads):
        here = pl.ds(head * span, span)
        merged[:, pl.ds(channels + head * depth, depth)] = (
            total[here, :] / jnp.sum(row_sum[here, :], axis=1, keepdims=True)
        ).astype(bf16)

    loads[7].wait()
    loads[8].wait()
    chunks = part_keep.shape[0]
    columns = part_keep.shape[3]

    def to_partner(k):
        return copy(part_send.at[k], part_come.at[k], pd_send.at[k], pd_recv.at[k], partner)

    def way(k):
        return 1 if k % 2 == 0 else -1

    def to_relay(k):
        return copy(pair.at[k, (x + 2) % 4], relay.at[k], relay_send.at[k], relay_recv.at[k], along_x(way(k)))

    def straight(k):
        return copy(
            pair.at[k, (x - way(k) + 4) % 4],
            come.at[k, 1],
            come_send.at[k, 1],
            come_recv.at[k, 1],
            along_x(-way(k)),
        )

    def relayed(k):
        return copy(passed.at[k], come.at[k, 0], come_send.at[k, 0], come_recv.at[k, 0], along_x(way(k)))

    def project(k):
        part = jnp.dot(
            merged[...], wout[:, pl.ds(k * columns, columns)], preferred_element_type=f32
        ).astype(bf16)
        part = part.reshape(4, 2, span // 8, columns)
        part_send[k] = jnp.where(core == 0, part[:, 1], part[:, 0])
        part_keep[k] = jnp.where(core == 0, part[:, 0], part[:, 1])
        to_partner(k).start()

    def add_pair(k):
        to_partner(k).wait_recv()
        pair[k] = (part_keep[k].astype(f32) + part_come[k].astype(f32)).astype(bf16)
        to_relay(k).start()
        straight(k).start()

    def add_relay(k):
        to_relay(k).wait_recv()
        mine = pair[k, (x + way(k) + 4) % 4].astype(f32)
        passed[k] = (mine + relay[k].astype(f32)).astype(bf16)
        relayed(k).start()

    def finish(k):
        straight(k).wait_recv()
        relayed(k).wait_recv()
        out_ref[:, pl.ds(k * columns, columns)] = (
            pair[k, x].astype(f32) + come[k, 0].astype(f32) + come[k, 1].astype(f32)
        ).astype(out_ref.dtype)

    for k in range(chunks + 2):
        if k < chunks:
            project(k)
        if 0 < k < chunks + 1:
            add_pair(k - 1)
        if k > 1:
            add_relay(k - 2)
    for k in range(chunks):
        finish(k)

    for one in first + second + crossing:
        one.wait_send()
    for k in range(chunks):
        to_partner(k).wait_send()
        to_relay(k).wait_send()
        straight(k).wait_send()
        relayed(k).wait_send()
    for j in range(1, ring):
        along(own.at[0, j], j, 1).wait_send()

    def sent(j, carry):
        for slot in range(1, half):
            right(own.at[slot, j], slot, j).wait_send()
            left(own.at[half + slot, j], half + slot, j).wait_send()
        for slot in range(ring):
            across(own.at[slot, j], slot, j).wait_send()
        return carry

    lax.fori_loop(0, ring, sent, 0)

    def sent_far(t, carry):
        right(own.at[half, 2 * t + 1], half, 2 * t + 1).wait_send()
        left(own.at[half, 2 * t], half, 2 * t).wait_send()
        return carry

    lax.fori_loop(0, half, sent_far, 0)


def shards(
    tokens,
    norm_gain,
    w_query,
    w_key,
    w_value,
    w_conv_value,
    w_conv_pre,
    w_conv_post,
    conv_taps,
    log_gate_cache,
    w_out_conv,
    w_out_attn,
):
    ring = math.isqrt(lax.axis_size("sp"))
    few, width = tokens.shape
    span = 8 * few
    depth = w_key.shape[1]
    channels = w_conv_post.shape[1]
    heads = w_query.shape[1] // depth
    block = span // 2
    chunks = 4
    columns = width // chunks
    bf16, f32 = jnp.bfloat16, jnp.float32
    dma = pltpu.SemaphoreType.DMA
    vmem = pltpu.VMEM
    here = pl.BlockSpec(memory_space=pltpu.VMEM)
    away = pl.BlockSpec(memory_space=pl.ANY)
    slots = vmem((ring, ring, 2, block, depth), bf16)
    return pl.pallas_call(
        functools.partial(layer_kernel, ring),
        out_shape=jax.ShapeDtypeStruct((few, width), bf16),
        in_specs=[here, here] + [away] * 6 + [here] + [away] * 3,
        out_specs=here,
        scratch_shapes=[
            vmem((8, few, width), bf16),
            vmem((width, heads * depth), bf16),
            vmem((width, 2 * depth), bf16),
            vmem((width, 3 * channels), bf16),
            vmem((channels + heads * depth, width), bf16),
            vmem(log_gate_cache.shape, f32),
            vmem((heads, 2 * ring * ring, block), f32),
            vmem((heads * span, depth), bf16),
            slots,
            slots,
            vmem((heads * span, 128), f32),
            vmem((heads * span, 128), f32),
            vmem((heads * span, depth), f32),
            vmem((16, channels), bf16),
            vmem((16, channels), bf16),
            vmem((span + 16, channels), f32),
            vmem((span, channels), bf16),
            vmem((span, channels + heads * depth), bf16),
            vmem((chunks, 4, few, columns), bf16),
            vmem((chunks, 4, few, columns), bf16),
            vmem((chunks, 4, few, columns), bf16),
            vmem((chunks, 4, few, columns), bf16),
            vmem((chunks, few, columns), bf16),
            vmem((chunks, few, columns), bf16),
            vmem((chunks, 2, few, columns), bf16),
            dma((9,)),
            dma((6,)),
            dma((6,)),
            dma((4,)),
            dma((4,)),
            dma((2,)),
            dma((ring,)),
            dma((ring, ring)),
            dma((ring, ring)),
            dma((ring, ring)),
            dma((ring, ring)),
            dma((ring, ring)),
            dma((chunks,)),
            dma((chunks,)),
            dma((chunks,)),
            dma((chunks,)),
            dma((chunks, 2)),
            dma((chunks, 2)),
        ],
        compiler_params=pltpu.CompilerParams(
            collective_id=0, has_side_effects=True, vmem_limit_bytes=60 << 20
        ),
        name="layer",
    )(
        tokens,
        norm_gain.reshape(1, width),
        w_query,
        w_key,
        w_value,
        w_conv_value,
        w_conv_pre,
        w_conv_post,
        conv_taps,
        log_gate_cache,
        w_out_conv,
        w_out_attn,
    )


def solution(mesh):
    placed = (
        P(("sp", "fs", "tp"), None),
        P(),
        P(None, ("fs", "tp")),
        P(None, "fs"),
        P(None, "fs"),
        P(None, ("fs", "tp")),
        P(None, ("fs", "tp")),
        P(None, ("fs", "tp")),
        P(),
        P(),
        P(("fs", "tp"), None),
        P(("fs", "tp"), None),
    )
    return jax.shard_map(
        shards, mesh=mesh, in_specs=placed, out_specs=P(("sp", "fs", "tp"), None), check_vma=False
    )
```

time: 112 us -> 79.1 us (0.71)
  Pallas kernels: 54.9 us -> 77 us
  blocking collectives: 19.8 us -> 0 us
  waiting for transfers between devices: 13.2 us -> 0 us
  starting transfers between devices: 11.7 us -> 0 us
  matrix products: 6.14 us -> 0 us
  other arithmetic: 4.81 us -> 0 us
    pallas_call x1, Pallas kernels: 54.9 us -> 77 us  [shards(): pl.pallas_call(functools.partial(layer_kernel, ring), out_shape=jax.Shape...]
    all_to_all x1 -> x0, blocking collectives: 19.8 us -> none  [sum_at_owner(): lax.all_to_all(tiles, axis, split_axis=0, concat_axis=0, tiled=True)]
    all_to_all x1 -> x0, waiting for transfers between devices: 13.2 us -> none  [sent_to_all(): lax.all_to_all(jnp.broadcast_to(value[None], (count, *value.shape)), axis...]
    all_to_all x1 -> x0, starting transfers between devices: 10.4 us -> none  [sent_to_all(): lax.all_to_all(jnp.broadcast_to(value[None], (count, *value.shape)), axis...]
    dot_general x6 -> x0, matrix products: 6.14 us -> none  [the longest x2 2.66 us: shards(): jnp.dot(own_rows, w, preferred_element_type=jnp.float32)]
    reduce_sum x2 -> x0, other arithmetic: 1.94 us -> none  [the longest x1 1.12 us: shards(): jnp.mean(float_rows * float_rows, axis=1, keepdims=True) + epsilon]
    convert_element_type x4 -> x0, other arithmetic: 1.74 us -> none  [the longest x1 1.01 us: shards(): normed_own = (scaled * norm_gain).astype(jnp.bfloat16)]
    unnamed x7 -> x1, local copies, waits for them, and re-layouts: 0.02 us -> 1.57 us
  transfers between devices with their start and end apart: 2 -> 0, of which waited for: 1 -> 0; matrix products, arithmetic and copies ran while one was open for 2% -> 0% of each run, Pallas kernels for 49% -> 0%
where the time goes in v2:
time: 79.1 us; the launch traced here: 78.6 us
  Pallas kernels  77 us (97%)
  local copies, waits for them, and re-layouts  1.57 us (2%)
    pallas_call x1, Pallas kernels, shards(): pl.pallas_call(functools.partial(layer_kernel, ring), out_shape=jax.Shape...  77 us

profile of v2, /device:TPU:1, one launch (start us, length us, event | category | flops | bytes accessed | tf_op | source)
XLA Modules:
  0.0 78.6 jit_solution(15645397981244812139)
XLA Ops:
  0.0 77.0 %layer.1 = bf16[32,2048]{1,0:T(8,128)(2,1)} custom-call(bf16[32,2048]{1,0:T(8,128)(2,1)} %tokens.1, f32[1,2048]{1,0:T(1,128)} %bitcast.1, bf16[2048,256]{1,0:T(8,128)(2,1)} %w_query.1, bf16[2048,128]{1,0:T(8,128)(2,1)} %w_key.1, bf16[2048,128]{1,0:T(8,128)(2,1)} %w_value.1, bf16[2048,128]{1,0:T(8,128)(2,1)} %w_conv_value.1, bf16[2048,128]{1,0:T(8,128)(2,1)} %w_conv_pre.1, ...), custom_call_target="tpu_custom_call" | custom-call | tf_op jit(solution)/shard_map/layer/pallas_call | solution.py:529
  77.1 1.6 %copy.14 = bf16[32,2048]{1,0:T(8,128)(2,1)} copy(bf16[32,2048]{1,0:T(8,128)(2,1)} %layer.1) | data formatting | bytes 262144

commit v3 on v2

--- a/solution.py
+++ b/solution.py
@@ -298,35 +298,55 @@
         y1 = (y - ds + origin * (ds - dp) + 2 * ring) % ring
         return z1 * ring + y1
 
-    def attend(buffer, pieces, origin, diagonal=False):
-        keys = jnp.concatenate([buffer[slot, j, 0] for slot, j in pieces], axis=0)
-        values = jnp.concatenate([buffer[slot, j, 1] for slot, j in pieces], axis=0)
-        for head in range(heads):
+    def attend(parts, pieces, diagonal=False):
+        blocks_of = [(buffer, slot, j, origin) for buffer, origin in parts for slot, j in pieces]
+
+        def score_of(unit):
+            head, some = unit
+            keys = jnp.concatenate([buffer[slot, j, 0] for buffer, slot, j, _ in some], axis=0)
+            return lax.dot_general(
+                q_ref[pl.ds(head * span, span), :],
+                keys,
+                (((1,), (1,)), ((), ())),
+                preferred_element_type=f32,
+            )
+
+        def absorb(score, unit):
+            head, some = unit
             here = pl.ds(head * span, span)
-            biases = []
-            for slot, j in pieces:
-                biases.append(bias_of[head, pl.ds(place(slot, j, origin) * 2 + origin, 1), :])
-            score = lax.dot_general(
-                q_ref[here, :], keys, (((1,), (1,)), ((), ())), preferred_element_type=f32
-            )
-            score = score * factor + jnp.concatenate(biases, axis=1)
-            if diagonal:
-                at = lax.broadcasted_iota(jnp.int32, score.shape, 0)
-                key = lax.broadcasted_iota(jnp.int32, score.shape, 1)
-                hidden = (key < block) & (key + origin * block > at)
-                score = jnp.where(hidden, masked_score, score)
+            values = jnp.concatenate([buffer[slot, j, 1] for buffer, slot, j, _ in some], axis=0)
+            parts_of = []
+            for n, (_, slot, j, origin) in enumerate(some):
+                bias = bias_of[head, pl.ds(place(slot, j, origin) * 2 + origin, 1), :]
+                part = score[:, n * block : (n + 1) * block] * factor + bias
+                if diagonal and slot == 0 and j == 0:
+                    at = lax.broadcasted_iota(jnp.int32, part.shape, 0)
+                    key = lax.broadcasted_iota(jnp.int32, part.shape, 1)
+                    part = jnp.where(key + origin * block > at, masked_score, part)
+                parts_of.append(part)
+            top = parts_of[0]
+            for part in parts_of[1:]:
+                top = jnp.maximum(top, part)
             old = row_max[here, :]
-            new = jnp.maximum(old, jnp.max(score, axis=1, keepdims=True))
+            new = jnp.maximum(old, jnp.max(top, axis=1, keepdims=True))
             rescale = jnp.exp2(old - new)
-            weight = jnp.exp2(score - jnp.concatenate([new] * (score.shape[1] // 128), axis=1))
-            lanes = weight[:, :128]
-            for i in range(1, score.shape[1] // 128):
-                lanes = lanes + weight[:, i * 128 : (i + 1) * 128]
+            weights = [jnp.exp2(part - new) for part in parts_of]
+            lanes = weights[0]
+            for weight in weights[1:]:
+                lanes = lanes + weight
             row_max[here, :] = new
             row_sum[here, :] = row_sum[here, :] * rescale + lanes
+            weight = jnp.concatenate([weight.astype(bf16) for weight in weights], axis=1)
             total[here, :] = total[here, :] * rescale + jnp.dot(
-                weight.astype(bf16), values, preferred_element_type=f32
+                weight, values, preferred_element_type=f32
             )
+
+        units = [(head, blocks_of) for head in range(heads)]
+        ahead = [score_of(unit) for unit in units[:1]]
+        for n, unit in enumerate(units):
+            if n + 1 < len(units):
+                ahead.append(score_of(units[n + 1]))
+            absorb(ahead[n], unit)
 
     order = arrival_order(ring)
     turns = len(order) // group
@@ -361,10 +381,9 @@
 
     def attend_turn(t, diagonal=False):
         pieces = [at_turn(t, i) for i in range(group)]
-        attend(own, pieces, core, diagonal)
         for slot, j in pieces:
             arrived_other(slot, j)
-        attend(other, pieces, far, diagonal)
+        attend(((own, core), (other, far)), pieces, diagonal)
 
     for i in range(1, group):
         slot, j = order[i]

time: 79.1 us -> 73.7 us (0.932)
  Pallas kernels: 77 us -> 71.6 us
    pallas_call x1, Pallas kernels: 77 us -> 71.6 us  [shards(): pl.pallas_call(functools.partial(layer_kernel, ring), out_shape=jax.Shape...]
where the time goes in v3:
time: 73.7 us; the launch traced here: 73.2 us
  Pallas kernels  71.6 us (97%)
  local copies, waits for them, and re-layouts  1.57 us (2%)
    pallas_call x1, Pallas kernels, shards(): pl.pallas_call(functools.partial(layer_kernel, ring), out_shape=jax.Shape...  71.6 us
    unnamed x1, local copies, waits for them, and re-layouts  1.57 us

profile of v3, /device:TPU:1, one launch (start us, length us, event | category | flops | bytes accessed | tf_op | source)
XLA Modules:
  0.0 73.2 jit_solution(10750170753013595885)
XLA Ops:
  0.0 71.6 %layer.1 = bf16[32,2048]{1,0:T(8,128)(2,1)} custom-call(bf16[32,2048]{1,0:T(8,128)(2,1)} %tokens.1, f32[1,2048]{1,0:T(1,128)} %bitcast.1, bf16[2048,256]{1,0:T(8,128)(2,1)} %w_query.1, bf16[2048,128]{1,0:T(8,128)(2,1)} %w_key.1, bf16[2048,128]{1,0:T(8,128)(2,1)} %w_value.1, bf16[2048,128]{1,0:T(8,128)(2,1)} %w_conv_value.1, bf16[2048,128]{1,0:T(8,128)(2,1)} %w_conv_pre.1, ...), custom_call_target="tpu_custom_call" | custom-call | tf_op jit(solution)/shard_map/layer/pallas_call | solution.py:548
  71.6 1.6 %copy.14 = bf16[32,2048]{1,0:T(8,128)(2,1)} copy(bf16[32,2048]{1,0:T(8,128)(2,1)} %layer.1) | data formatting | bytes 262144

commit v4 on v3

--- a/solution.py
+++ b/solution.py
@@ -478,13 +478,13 @@
             pair[k, x].astype(f32) + come[k, 0].astype(f32) + come[k, 1].astype(f32)
         ).astype(out_ref.dtype)
 
-    for k in range(chunks + 2):
+    for k in range(chunks + 1):
         if k < chunks:
             project(k)
-        if 0 < k < chunks + 1:
+        if k > 0:
             add_pair(k - 1)
-        if k > 1:
-            add_relay(k - 2)
+    for k in range(chunks):
+        add_relay(k)
     for k in range(chunks):
         finish(k)
 

time: 73.7 us -> 71.1 us (0.965)
  Pallas kernels: 71.6 us -> 69.3 us
    pallas_call x1, Pallas kernels: 71.6 us -> 69.3 us  [shards(): pl.pallas_call(functools.partial(layer_kernel, ring), out_shape=jax.Shape...]
where the time goes in v4:
time: 71.1 us; the launch traced here: 70.9 us
  Pallas kernels  69.3 us (97%)
  local copies, waits for them, and re-layouts  1.57 us (2%)
    pallas_call x1, Pallas kernels, shards(): pl.pallas_call(functools.partial(layer_kernel, ring), out_shape=jax.Shape...  69.3 us
    unnamed x1, local copies, waits for them, and re-layouts  1.57 us

profile of v4, /device:TPU:1, one launch (start us, length us, event | category | flops | bytes accessed | tf_op | source)
XLA Modules:
  0.0 70.9 jit_solution(18276924028034331234)
XLA Ops:
  0.0 69.3 %layer.1 = bf16[32,2048]{1,0:T(8,128)(2,1)} custom-call(bf16[32,2048]{1,0:T(8,128)(2,1)} %tokens.1, f32[1,2048]{1,0:T(1,128)} %bitcast.1, bf16[2048,256]{1,0:T(8,128)(2,1)} %w_query.1, bf16[2048,128]{1,0:T(8,128)(2,1)} %w_key.1, bf16[2048,128]{1,0:T(8,128)(2,1)} %w_value.1, bf16[2048,128]{1,0:T(8,128)(2,1)} %w_conv_value.1, bf16[2048,128]{1,0:T(8,128)(2,1)} %w_conv_pre.1, ...), custom_call_target="tpu_custom_call" | custom-call | tf_op jit(solution)/shard_map/layer/pallas_call | solution.py:548
  69.3 1.6 %copy.14 = bf16[32,2048]{1,0:T(8,128)(2,1)} copy(bf16[32,2048]{1,0:T(8,128)(2,1)} %layer.1) | data formatting | bytes 262144

commit v5 on v4

--- a/solution.py
+++ b/solution.py
@@ -20,7 +20,7 @@
     for slot in range(ring):
         hops = slot if slot <= half else slot - half
         for j in range(ring):
-            pieces.append((hops + (j + 1) // 2, hops, slot, j))
+            pieces.append((10 * hops + 8 * ((j + 1) // 2), hops, slot, j))
     return [(slot, j) for _, _, slot, j in sorted(pieces)]
 
 
@@ -398,15 +398,6 @@
             right(here, slot + 1, j).start()
         across(here, slot, j).start()
     pass_on(jnp.int32(1))
-    attend_turn(0, diagonal=True)
-
-    def turn(t, carry):
-        pass_on(t)
-        attend_turn(t - 1)
-        return carry
-
-    lax.fori_loop(2, turns, turn, 0)
-
     shift.wait()
     extended[pl.ds(0, edge), :] = jnp.where(sp == 0, 0.0, halo[...].astype(f32))
     at = pl.multiple_of(device * channels, channels)
@@ -417,6 +408,15 @@
         conv_sum = conv_sum + tap_rows[n : n + 1] * extended[pl.ds(edge - count + 1 + n, span), :]
     merged[:, pl.ds(0, channels)] = (gate_after[...].astype(f32) * conv_sum).astype(bf16)
 
+    attend_turn(0, diagonal=True)
+
+    def turn(t, carry):
+        pass_on(t)
+        attend_turn(t - 1)
+        return carry
+
+    lax.fori_loop(2, turns, turn, 0)
+
     attend_turn(turns - 1)
     for head in range(heads):
         here = pl.ds(head * span, span)
@@ -483,18 +483,8 @@
             project(k)
         if k > 0:
             add_pair(k - 1)
-    for k in range(chunks):
-        add_relay(k)
-    for k in range(chunks):
-        finish(k)
-
     for one in first + second + crossing:
         one.wait_send()
-    for k in range(chunks):
-        to_partner(k).wait_send()
-        to_relay(k).wait_send()
-        straight(k).wait_send()
-        relayed(k).wait_send()
     for j in range(1, ring):
         along(own.at[0, j], j, 1).wait_send()
 
@@ -514,6 +504,17 @@
         return carry
 
     lax.fori_loop(0, half, sent_far, 0)
+
+    for k in range(chunks):
+        add_relay(k)
+    for k in range(chunks):
+        finish(k)
+
+    for k in range(chunks):
+        to_partner(k).wait_send()
+        to_relay(k).wait_send()
+        straight(k).wait_send()
+        relayed(k).wait_send()
 
 
 def shards(

time: 71.1 us -> 70.6 us (level)
  no operation moved by 1% of the time
where the time goes in v5:
time: 70.6 us; the launch traced here: 70.5 us
  Pallas kernels  68.9 us (98%)
  local copies, waits for them, and re-layouts  1.57 us (2%)
    pallas_call x1, Pallas kernels, shards(): pl.pallas_call(functools.partial(layer_kernel, ring), out_shape=jax.Shape...  68.9 us
    unnamed x1, local copies, waits for them, and re-layouts  1.57 us

profile of v5, /device:TPU:1, one launch (start us, length us, event | category | flops | bytes accessed | tf_op | source)
XLA Modules:
  0.0 70.5 jit_solution(5904065805886616951)
XLA Ops:
  0.0 68.9 %layer.1 = bf16[32,2048]{1,0:T(8,128)(2,1)} custom-call(bf16[32,2048]{1,0:T(8,128)(2,1)} %tokens.1, f32[1,2048]{1,0:T(1,128)} %bitcast.1, bf16[2048,256]{1,0:T(8,128)(2,1)} %w_query.1, bf16[2048,128]{1,0:T(8,128)(2,1)} %w_key.1, bf16[2048,128]{1,0:T(8,128)(2,1)} %w_value.1, bf16[2048,128]{1,0:T(8,128)(2,1)} %w_conv_value.1, bf16[2048,128]{1,0:T(8,128)(2,1)} %w_conv_pre.1, ...), custom_call_target="tpu_custom_call" | custom-call | tf_op jit(solution)/shard_map/layer/pallas_call | solution.py:549
  68.9 1.6 %copy.14 = bf16[32,2048]{1,0:T(8,128)(2,1)} copy(bf16[32,2048]{1,0:T(8,128)(2,1)} %layer.1) | data formatting | bytes 262144
